TPU v7x, 32 devices: a whole 2x2x4 slice. The times are simulated.
32 devices in a mesh: sp: 8 (over z, x), dp: 4 (over y, core).
Axes of the slice: x: 2, y: 2, z: 4, core: 2. Of those that a mesh axis runs over, the one named last changes fastest.
Arguments:
- tokens: bfloat16 [4, 4096, 4096], P('dp', 'sp'), may hold values from -6 to 6
- documents: int32 [4, 4096], P('dp', 'sp'), may hold values from 0 to 7, never falling along the last dimension, each value on 1 to 1024 neighbouring positions
- value_weight: bfloat16 [4096, 2048], P(('sp', 'dp')), may hold values from -0.09375 to 0.09375
- gate_weight: bfloat16 [4096, 2048], P(('sp', 'dp')), may hold values from -0.09375 to 0.09375
- conv_weight: bfloat16 [31, 2048], replicated, may hold values from -1 to 1
- norm_gain: float32 [2048], replicated, may hold values from 0.1 to 1.9
- norm_bias: float32 [2048], replicated, may hold values from -2 to 2
Outputs:
- activated: bfloat16 [4, 4096, 2048], P('dp', 'sp')
Inputs may be any that keep to these rules, and one draw needn't show every extreme that they name: `documents`: document numbers never fall along a sequence, run from 0 to 7, and each document covers 1 to 1024 positions.
All inputs are finite; a program needn't handle non-finite values.
Results may differ from a plain program's by a relative error of at most 0.0064.
Values may be sent and summed in bfloat16 or wider, within the bound.
A program may use at most 192 MiB of HBM per device.

v0:
```python
import functools

import jax
import jax.numpy as jnp
from jax import lax
from jax.experimental import pallas as pl
from jax.experimental.pallas import tpu as pltpu
from jax.sharding import PartitionSpec as P

KERNEL = 31
BLOCKS = 4
HALO = 32
MESH = pl.DeviceIdType.MESH


def gather_kernel(
    side, tall, tok_hbm, own_hbm, glu_ref, weights, tok, send, recv, cross, begin, halo
):
    sp, dp = lax.axis_index("sp"), lax.axis_index("dp")
    sp_size = lax.axis_size("sp")
    core, y = lax.rem(dp, 2), lax.div(dp, 2)
    z, x = lax.div(sp, side), lax.rem(sp, side)
    flip = core == 1
    u, v = jnp.where(flip, y, x), jnp.where(flip, x, y)
    half = own_hbm.shape[2]
    depth = 2 * half
    count = tok_hbm.shape[0]
    sub = tall // 2
    columns = weights.shape[3] // sub
    wide = columns // 2
    other = {"sp": sp, "dp": y * 2 + (1 - core)}

    def device(dz, du, dv):
        dx, dy = jnp.where(flip, dv, du), jnp.where(flip, du, dv)
        return {"sp": dz * side + dx, "dp": dy * 2 + core}

    def number(pz, pu, pv):
        px, py = jnp.where(flip, pv, pu), jnp.where(flip, pu, pv)
        return (pz * side + px) * side + py

    def piece(plane, block, q):
        return weights.at[plane, block, pl.ds(pl.multiple_of(q * depth, depth), depth), :]

    def link(kind, block, q, target):
        return pltpu.make_async_remote_copy(
            src_ref=piece(core, block, q),
            dst_ref=piece(core, block, q),
            send_sem=send.at[kind, block, q],
            recv_sem=recv.at[block, q],
            device_id=target,
            device_id_type=MESH,
        )

    def hand_over(plane, block, q):
        return pltpu.make_async_remote_copy(
            src_ref=piece(plane, block, q),
            dst_ref=piece(plane, block, q),
            send_sem=send.at[6, block, q],
            recv_sem=cross.at[block, q],
            device_id=other,
            device_id_type=MESH,
        )

    def routes(block, pz, pu, pv, act):
        q = number(pz, pu, pv)
        tall_first = block == 1
        home_u, home_v, home_z = u == pu, v == pv, z == pz
        along_z = home_v & (home_u | jnp.logical_not(tall_first))
        along_u = home_v & (home_z | tall_first)
        ways = (
            (along_z & (z >= pz) & (z + 1 < tall), (z + 1, u, v)),
            (along_z & (z <= pz) & (z > 0), (z - 1, u, v)),
            (along_u & (u >= pu) & (u + 1 < side), (z, u + 1, v)),
            (along_u & (u <= pu) & (u > 0), (z, u - 1, v)),
            ((v >= pv) & (v + 1 < side), (z, u, v + 1)),
            ((v <= pv) & (v > 0), (z, u, v - 1)),
        )
        for kind, (taken, target) in enumerate(ways):

            @pl.when(taken)
            def _(kind=kind, target=target):
                act(link(kind, block, q, device(*target)))

        @pl.when(jnp.logical_not(home_u & home_v & home_z))
        def _():
            act(hand_over(core, block, q))

    def pass_on(block, pz, pu, pv):
        routes(block, pz, pu, pv, lambda copy: copy.start())

    def arrived(block, pz, pu, pv):
        link(0, block, number(pz, pu, pv), other).wait_recv()
        pass_on(block, pz, pu, pv)

    low = jnp.minimum(z, tall - 1 - z)

    def near(k):
        step = jnp.where(lax.rem(k, 2) == 1, low - lax.div(k + 1, 2), low + lax.div(k, 2))
        at = jnp.where(k <= 2 * low, step, k)
        return jnp.where(z == low, at, tall - 1 - at)

    barrier = pltpu.get_barrier_semaphore()
    greeted = jnp.int32(1)
    pl.semaphore_signal(barrier, inc=1, device_id=other, device_id_type=MESH)
    for there, target in (
        (z + 1 < tall, device(z + 1, u, v)),
        (z > 0, device(z - 1, u, v)),
        (u + 1 < side, device(z, u + 1, v)),
        (u > 0, device(z, u - 1, v)),
        (v + 1 < side, device(z, u, v + 1)),
        (v > 0, device(z, u, v - 1)),
        (sp + 1 < sp_size, {"sp": sp + 1, "dp": dp}),
        (sp > 0, {"sp": sp - 1, "dp": dp}),
    ):
        greeted = greeted + there.astype(jnp.int32)

        @pl.when(there)
        def _(target=target):
            pl.semaphore_signal(barrier, inc=1, device_id=target, device_id_type=MESH)

    pl.semaphore_wait(barrier, greeted)

    here = (z * side + x) * side + y
    own_rows = weights.at[
        :, :, pl.ds(pl.multiple_of(here * depth + core * half, half), half), :
    ]
    to_other = pltpu.make_async_remote_copy(
        src_ref=own_hbm,
        dst_ref=own_rows,
        send_sem=begin.at[0],
        recv_sem=begin.at[1],
        device_id=other,
        device_id_type=MESH,
    )
    to_other.start()
    keep = pltpu.make_async_copy(own_hbm, own_rows, begin.at[2])
    keep.start()
    load = pltpu.make_async_copy(tok_hbm, tok.at[pl.ds(HALO, count), :], begin.at[3])
    load.start()
    tail = pltpu.make_async_remote_copy(
        src_ref=tok_hbm.at[pl.ds(count - HALO, HALO), :],
        dst_ref=tok.at[pl.ds(0, HALO), :],
        send_sem=halo.at[0],
        recv_sem=halo.at[1],
        device_id={"sp": lax.rem(sp + 1, sp_size), "dp": dp},
        device_id_type=MESH,
    )

    @pl.when(sp + 1 < sp_size)
    def _():
        tail.start()

    @pl.when(sp == 0)
    def _():
        tok[pl.ds(0, HALO), :] = jnp.zeros((HALO, tok.shape[1]), tok.dtype)

    keep.wait()
    to_other.wait_recv()
    pass_on(0, z, u, v)
    load.wait()

    @pl.when(sp > 0)
    def _():
        tail.wait_recv()

    def tick(at, carry):
        block, k = lax.div(at, tall), lax.rem(at, tall)

        @pl.when((block < BLOCKS) & (k > 0))
        def _():
            arrived(block, near(k), u, v)

        @pl.when((block + 1 < BLOCKS) & (k == 0))
        def _():
            pass_on(block + 1, z, u, v)

        second = jnp.maximum(at - 1, 0)
        block2, k2 = lax.div(second, tall), lax.rem(second, tall)

        @pl.when((at >= 1) & (block2 < BLOCKS))
        def _():
            @pl.loop(1, side)
            def _(du):
                arrived(block2, near(k2), lax.rem(u + du, side), v)

        third = jnp.maximum(at - 2, 0)
        block3, k3 = lax.div(third, tall), lax.rem(third, tall)

        @pl.when((at >= 2) & (block3 < BLOCKS))
        def _():
            @pl.loop(0, side)
            def _(du):
                @pl.loop(1, side)
                def _(dv):
                    arrived(block3, near(k3), lax.rem(u + du, side), lax.rem(v + dv, side))

        late = jnp.maximum(at - tall - 2, 0)
        block4, k4 = lax.div(late, tall), lax.rem(late, tall)

        @pl.when((at >= tall + 2) & (k4 == 0))
        def _():
            @pl.loop(0, tall * side * side)
            def _(q):
                @pl.when(q != here)
                def _():
                    hand_over(1 - core, block4, q).wait_recv()

        @pl.when(at >= tall + 2)
        def _():
            plane, part = lax.div(k4, sub), lax.rem(k4, sub)
            held = weights[
                plane, block4, :, pl.ds(pl.multiple_of(part * columns, columns), columns)
            ]
            both = jnp.dot(tok[...], held, preferred_element_type=jnp.float32)
            value = both[:, :wide].astype(jnp.bfloat16).astype(jnp.float32)
            gate = both[:, wide:].astype(jnp.bfloat16).astype(jnp.float32)
            first = ((plane * BLOCKS + block4) * sub + part) * wide
            glu_ref[:, pl.ds(pl.multiple_of(first, wide), wide)] = (
                value * jax.nn.sigmoid(gate)
            ).astype(jnp.bfloat16)

        return carry

    lax.fori_loop(0, BLOCKS * tall + tall + 2, tick, 0)

    @pl.loop(0, BLOCKS)
    def _(block):
        @pl.loop(0, tall)
        def _(pz):
            @pl.loop(0, side)
            def _(pu):
                @pl.loop(0, side)
                def _(pv):
                    routes(block, pz, pu, pv, lambda copy: copy.wait_send())

    to_other.wait_send()

    @pl.when(sp + 1 < sp_size)
    def _():
        tail.wait_send()


def gated_product(rows, value_weight, gate_weight):
    side = lax.axis_size("dp") // 2
    tall = lax.axis_size("sp") // side
    count, width = rows.shape
    depth, channels = value_weight.shape
    wide = channels // (BLOCKS * tall)
    cut = (depth, 2, BLOCKS, tall // 2, 1, wide)
    own = jnp.concatenate([value_weight.reshape(cut), gate_weight.reshape(cut)], axis=4)
    own = own.transpose(1, 2, 0, 3, 4, 5).reshape(2, BLOCKS, depth, channels // BLOCKS)
    pieces = tall * side * side
    return pl.pallas_call(
        functools.partial(gather_kernel, side, tall),
        out_shape=jax.ShapeDtypeStruct((HALO + count, channels), jnp.bfloat16),
        in_specs=[pl.BlockSpec(memory_space=pl.ANY)] * 2,
        out_specs=pl.BlockSpec(memory_space=pltpu.VMEM),
        scratch_shapes=[
            pltpu.VMEM((2, BLOCKS, width, channels // BLOCKS), jnp.bfloat16),
            pltpu.VMEM((HALO + count, width), jnp.bfloat16),
            pltpu.SemaphoreType.DMA((7, BLOCKS, pieces)),
            pltpu.SemaphoreType.DMA((BLOCKS, pieces)),
            pltpu.SemaphoreType.DMA((BLOCKS, pieces)),
            pltpu.SemaphoreType.DMA((4,)),
            pltpu.SemaphoreType.DMA((2,)),
        ],
        compiler_params=pltpu.CompilerParams(
            collective_id=0, has_side_effects=True, vmem_limit_bytes=56 * 1024 * 1024
        ),
    )(rows, own)


def passed_along(block, axis, distance):
    devices = range(lax.axis_size(axis))
    route = [(i - distance, i) for i in devices if i - distance in devices]
    return lax.ppermute(block, axis, route)


def mix_kernel(glu_ref, reach_ref, taps_ref, gain_ref, bias_ref, out_ref, mixed):
    rows, channels = out_ref.shape
    top = pl.multiple_of(pl.program_id(0) * rows, rows)
    reach = reach_ref[...]

    @pl.loop(0, channels // 128)
    def _(lane):
        lanes = pl.ds(pl.multiple_of(lane * 128, 128), 128)
        window = glu_ref[pl.ds(top, rows + HALO), lanes].astype(jnp.float32)
        total = jnp.zeros((rows, 128), jnp.float32)
        for shift in range(8):
            held = window if shift == 0 else window[shift : shift + rows + HALO - 8]
            for offset in range(shift, HALO + 1, 8):
                lag = HALO - offset
                if lag < KERNEL:
                    moved = held[offset - shift : offset - shift + rows]
                    moved = jnp.where(reach >= lag, moved, 0.0)
                    total = total + moved * taps_ref[lag : lag + 1, lanes]
        mixed[:, lanes] = total.astype(jnp.bfloat16).astype(jnp.float32)

    wide = mixed[...]
    center = wide - jnp.mean(wide, axis=-1, keepdims=True)
    spread = jnp.mean(center * center, axis=-1, keepdims=True)
    normed = center * lax.rsqrt(spread + 1e-06) * gain_ref[...] + bias_ref[...]
    out_ref[...] = (normed * jax.nn.sigmoid(normed)).astype(jnp.bfloat16)


def mix_and_finish(glu, reach, taps, norm_gain, norm_bias):
    channels = glu.shape[1]
    count = reach.shape[0]
    rows = 64
    return pl.pallas_call(
        mix_kernel,
        grid=(count // rows,),
        out_shape=jax.ShapeDtypeStruct((count, channels), jnp.bfloat16),
        in_specs=[
            pl.BlockSpec(glu.shape, lambda i: (0, 0)),
            pl.BlockSpec((rows, 128), lambda i: (i, 0)),
            pl.BlockSpec(taps.shape, lambda i: (0, 0)),
            pl.BlockSpec((1, channels), lambda i: (0, 0)),
            pl.BlockSpec((1, channels), lambda i: (0, 0)),
        ],
        out_specs=pl.BlockSpec((rows, channels), lambda i: (i, 0)),
        scratch_shapes=[pltpu.VMEM((rows, channels), jnp.float32)],
    )(glu, reach, taps, norm_gain[None], norm_bias[None])


def per_device(tokens, documents, value_weight, gate_weight, conv_weight, norm_gain, norm_bias):
    batch, count, width = tokens.shape
    channels = value_weight.shape[1]
    lead = KERNEL - 1
    rows = tokens.reshape(batch * count, width)
    docs = documents.reshape(count)
    before_docs = passed_along(docs[count - lead :], "sp", 1)
    before_docs = jnp.where(lax.axis_index("sp") == 0, -1, before_docs)
    docs_wide = jnp.concatenate([before_docs, docs])
    reach = jnp.zeros((count,), jnp.int32)
    for lag in range(1, KERNEL):
        reach = reach + (docs_wide[lead - lag : lead - lag + count] == docs).astype(jnp.int32)
    reach = jnp.broadcast_to(reach[:, None], (count, 128))
    glu = gated_product(rows, value_weight, gate_weight)
    taps = jnp.pad(conv_weight.astype(jnp.float32), ((0, 1), (0, 0)))
    out = mix_and_finish(glu, reach, taps, norm_gain, norm_bias)
    return out.reshape(batch, count, channels)


def solution(mesh):
    return jax.shard_map(
        per_device,
        mesh=mesh,
        in_specs=(
            P("dp", "sp", None),
            P("dp", "sp"),
            P(("sp", "dp"), None),
            P(("sp", "dp"), None),
            P(),
            P(),
            P(),
        ),
        out_specs=P("dp", "sp", None),
        check_vma=False,
    )
```

profile of v0, /device:TPU:0, one launch (start us, length us, event | category | flops | bytes accessed | tf_op | source)
XLA Modules:
  0.0 204.5 jit_solution(9567032164387596264)
XLA Ops:
  0.0 0.0 copy-start
  0.0 0.8 slice_bitcast_fusion
  0.8 4.9 %collective-permute-start = (s32[30]{0:T(128)S(1)}, s32[30]{0:T(128)S(1)}, u32[]{:S(2)}, u32[]{:S(2)}) collective-permute-start(s32[30]{0:T(128)S(1)} %slice_bitcast_fusion), channel_id=1, source_target_pairs={{0,4},{4,8},{8,12},{12,16},{16,20},{20,24},{24,28},{1,5},{5,9},{9,... | collective-permute-start | bytes 368 | tf_op jit(solution)/shard_map/ppermute | solution.py:276
  5.7 1.6 pad_convert_fusion.taps_ref
  7.3 1.4 reshape.21
  8.7 1.1 copy.8
  9.8 0.0 copy-done
  9.8 0.4 reshape.22
  10.2 1.1 copy.9
  11.2 2.4 %maximum_bitcast_fusion = bf16[2,4,128,2,2,128]{5,4,3,2,1,0:T(2,128)(2,1)S(1)} fusion(bf16[128,2,4,2,1,128]{5,4,3,0,2,1:T(2,128)(2,1)S(1)} %copy.9, bf16[128,2,4,2,1,128]{5,4,3,0,2,1:T(2,128)(2,1)S(1)} %copy.8), kind=kLoop, calls=%fused_computation | loop fusion | flops 2097152 | bytes 2097152 | tf_op jit(solution)/shard_map/transpose | solution.py:251
  13.7 1.2 reshape.23.own_hbm
  14.9 0.0 copy-start.1
  14.9 162.2 %shard_map.73.glu_ref = bf16[544,2048]{1,0:T(8,128)(2,1)} custom-call(bf16[512,4096]{1,0:T(8,128)(2,1)} %bitcast.9, bf16[2,4,128,512]{3,2,1,0:T(8,128)(2,1)} %reshape.23.own_hbm), custom_call_target="tpu_custom_call" | custom-call | tf_op jit(solution)/shard_map/pallas_call | solution.py:253
  177.1 0.0 collective-permute-done
  177.1 0.0 copy-done.1
  177.1 0.1 pad_add_fusion
  177.2 0.1 convert_add_fusion
  177.3 0.8 broadcast_in_dim.17.reach_ref
  178.2 26.3 %shard_map.74 = bf16[512,2048]{1,0:T(8,128)(2,1)} custom-call(bf16[544,2048]{1,0:T(8,128)(2,1)} %shard_map.73.glu_ref, s32[512,128]{1,0:T(8,128)} %broadcast_in_dim.17.reach_ref, f32[32,2048]{1,0:T(8,128)} %pad_convert_fusion.taps_ref, f32[1,2048]{1,0:T(1,128)} %bitcast.10, f32[1,2048]{1,0:T(1,128)} %bitcast.11), custom_call_target="tpu_custom_call" | custom-call | tf_op jit(solution)/shard_map/pallas_call | solution.py:310
  (1 shorter events, 0.0 us)
Async XLA Ops:
  0.0 9.8 %copy-start = (bf16[128,2048]{1,0:T(8,128)(2,1)S(1)}, bf16[128,2048]{1,0:T(8,128)(2,1)}, u32[]{:S(2)}) copy-start(bf16[128,2048]{1,0:T(8,128)(2,1)} %param.10) | copy-start | bytes 1572868
  0.8 176.3 %collective-permute-start = (s32[30]{0:T(128)S(1)}, s32[30]{0:T(128)S(1)}, u32[]{:S(2)}, u32[]{:S(2)}) collective-permute-start(s32[30]{0:T(128)S(1)} %slice_bitcast_fusion), channel_id=1, source_target_pairs={{0,4},{4,8},{8,12},{12,16},{16,20},{20,24},{24,28},{1,5},{5,9},{9,... | collective-permute-start | bytes 368 | tf_op jit(solution)/shard_map/ppermute | solution.py:276
  14.9 162.2 %copy-start.1 = (s32[1,512]{1,0:T(1,128)S(1)}, s32[1,512]{1,0:T(1,128)}, u32[]{:S(2)}) copy-start(s32[1,512]{1,0:T(1,128)} %param.8) | copy-start | bytes 6148
where the time goes:
time: 205 us; the launch traced here: 204 us
  Pallas kernels  188 us (92%)
  local copies, waits for them, and re-layouts  6.77 us (3%)
  starting transfers between devices  4.86 us (2%)
  other arithmetic  4.25 us (2%)
    pallas_call x1, Pallas kernels, gated_product(): pl.pallas_call(functools.partial(gather_kernel, side, tall), out_shape=ja...  162 us
    pallas_call x1, Pallas kernels, mix_and_finish(): pl.pallas_call(mix_kernel, grid=(count // rows,), out_shape=jax.ShapeDtyp...  26.3 us
    ppermute x1, starting transfers between devices, passed_along(): return lax.ppermute(block, axis, route)  4.86 us
  transfers between devices with their start and end apart: 1, of which 0 were waited for; matrix products, arithmetic and copies ran while one was open for 5% of the time, Pallas kernels for 79%

commit v1 on v0

v1 whole, which is shorter than its diff:
```python
import functools

import jax
import jax.numpy as jnp
from jax import lax
from jax.experimental import pallas as pl
from jax.experimental.pallas import tpu as pltpu
from jax.sharding import PartitionSpec as P

KERNEL = 31
HALO = 32
LANES = 128
TILE = 64
AHEAD = 1
KEPT = 5
MESH = pl.DeviceIdType.MESH


def fused_kernel(
    side, tall, blocks, tok_hbm, docs_hbm, value_hbm, gate_hbm, conv_ref, mixed_ref,
    weights, tok, docs, taps, shifted, far, near_by, send, recv, cross, own, begin, halo
):
    sp, dp = lax.axis_index("sp"), lax.axis_index("dp")
    sp_size = lax.axis_size("sp")
    core, y = lax.rem(dp, 2), lax.div(dp, 2)
    z, x = lax.div(sp, side), lax.rem(sp, side)
    flip = core == 1
    u, v = jnp.where(flip, y, x), jnp.where(flip, x, y)
    depth = value_hbm.shape[0]
    count = tok_hbm.shape[0]
    parts = tall // 2
    second_start, third_start = 2, 6
    late_start = third_start + tall
    other = {"sp": sp, "dp": y * 2 + (1 - core)}
    here = (z * side + x) * side + y

    def device(dz, du, dv):
        dx, dy = jnp.where(flip, dv, du), jnp.where(flip, du, dv)
        return {"sp": dz * side + dx, "dp": dy * 2 + core}

    def number(pz, pu, pv):
        px, py = jnp.where(flip, pv, pu), jnp.where(flip, pu, pv)
        return (pz * side + px) * side + py

    def piece(which, block, q):
        return weights.at[
            block, pl.ds(pl.multiple_of((q * 2 + which) * depth, depth), depth), :
        ]

    def link(kind, block, q, target):
        return pltpu.make_async_remote_copy(
            src_ref=piece(core, block, q),
            dst_ref=piece(core, block, q),
            send_sem=send.at[kind, lax.rem(block, KEPT), q],
            recv_sem=recv.at[block, q],
            device_id=target,
            device_id_type=MESH,
        )

    def hand_over(which, block, q):
        return pltpu.make_async_remote_copy(
            src_ref=piece(which, block, q),
            dst_ref=piece(which, block, q),
            send_sem=send.at[6, lax.rem(block, KEPT), q],
            recv_sem=cross.at[block, q],
            device_id=other,
            device_id_type=MESH,
        )

    def routes(block, pz, pu, pv, act):
        q = number(pz, pu, pv)
        tall_first = (block == 1) | (block == 4) | (block == 6)
        home_u, home_v, home_z = u == pu, v == pv, z == pz
        along_z = home_v & (home_u | jnp.logical_not(tall_first))
        along_u = home_v & (home_z | tall_first)
        ways = (
            (along_z & (z >= pz) & (z + 1 < tall), (z + 1, u, v)),
            (along_z & (z <= pz) & (z > 0), (z - 1, u, v)),
            (along_u & (u >= pu) & (u + 1 < side), (z, u + 1, v)),
            (along_u & (u <= pu) & (u > 0), (z, u - 1, v)),
            ((v >= pv) & (v + 1 < side), (z, u, v + 1)),
            ((v <= pv) & (v > 0), (z, u, v - 1)),
        )
        for kind, (taken, target) in enumerate(ways):

            @pl.when(taken)
            def _(kind=kind, target=target):
                act(link(kind, block, q, device(*target)))

        act(hand_over(core, block, q))

    def pass_on(block, pz, pu, pv):
        routes(block, pz, pu, pv, lambda copy: copy.start())

    def arrived(block, pz, pu, pv):
        link(0, block, number(pz, pu, pv), other).wait_recv()
        pass_on(block, pz, pu, pv)

    low = jnp.minimum(z, tall - 1 - z)

    def near(k):
        step = jnp.where(lax.rem(k, 2) == 1, low - lax.div(k + 1, 2), low + lax.div(k, 2))
        at = jnp.where(k <= 2 * low, step, k)
        return jnp.where(z == low, at, tall - 1 - at)

    def own_copies(block):
        rows = pl.ds(pl.multiple_of((here * 2 + core) * depth, depth), depth)
        for part in range(parts):
            first = pl.multiple_of((block * parts + part) * LANES, LANES)
            for half, source in enumerate((value_hbm, gate_hbm)):
                yield pltpu.make_async_copy(
                    source.at[:, pl.ds(first, LANES)],
                    weights.at[block, rows, pl.ds((2 * part + half) * LANES, LANES)],
                    own.at[block, 2 * part + half],
                )

    def send_own(block):
        for copy in own_copies(block):
            copy.wait()
        pass_on(block, z, u, v)

    @pl.loop(0, blocks)
    def _(block):
        for copy in own_copies(block):
            copy.start()

    load = pltpu.make_async_copy(tok_hbm, tok.at[pl.ds(HALO, count), :], begin.at[0])
    load.start()
    read = pltpu.make_async_copy(docs_hbm, docs.at[:, pl.ds(LANES, count)], begin.at[1])
    read.start()

    barrier = pltpu.get_barrier_semaphore()
    greeted = jnp.int32(1)
    pl.semaphore_signal(barrier, inc=1, device_id=other, device_id_type=MESH)
    for there, target in (
        (z + 1 < tall, device(z + 1, u, v)),
        (z > 0, device(z - 1, u, v)),
        (u + 1 < side, device(z, u + 1, v)),
        (u > 0, device(z, u - 1, v)),
        (v + 1 < side, device(z, u, v + 1)),
        (v > 0, device(z, u, v - 1)),
        (sp + 1 < sp_size, {"sp": sp + 1, "dp": dp}),
        (sp > 0, {"sp": sp - 1, "dp": dp}),
    ):
        greeted = greeted + there.astype(jnp.int32)

        @pl.when(there)
        def _(target=target):
            pl.semaphore_signal(barrier, inc=1, device_id=target, device_id_type=MESH)

    pl.semaphore_wait(barrier, greeted)

    following = {"sp": lax.rem(sp + 1, sp_size), "dp": dp}
    tail = pltpu.make_async_remote_copy(
        src_ref=tok_hbm.at[pl.ds(count - HALO, HALO), :],
        dst_ref=tok.at[pl.ds(0, HALO), :],
        send_sem=halo.at[0],
        recv_sem=halo.at[1],
        device_id=following,
        device_id_type=MESH,
    )
    docs_tail = pltpu.make_async_remote_copy(
        src_ref=docs_hbm.at[:, pl.ds(count - LANES, LANES)],
        dst_ref=docs.at[:, pl.ds(0, LANES)],
        send_sem=halo.at[2],
        recv_sem=halo.at[3],
        device_id=following,
        device_id_type=MESH,
    )

    @pl.loop(0, AHEAD)
    def _(block):
        send_own(block)

    @pl.when(sp + 1 < sp_size)
    def _():
        tail.start()
        docs_tail.start()

    @pl.when(sp == 0)
    def _():
        tok[pl.ds(0, HALO), :] = jnp.zeros((HALO, tok.shape[1]), tok.dtype)
        docs[:, pl.ds(0, LANES)] = jnp.full((1, LANES), -1, jnp.int32)

    taps[pl.ds(0, KERNEL), :] = conv_ref[...].astype(jnp.float32)

    def prepare():
        load.wait()
        read.wait()

        @pl.when(sp > 0)
        def _():
            tail.wait_recv()
            docs_tail.wait_recv()

        column = jnp.broadcast_to(docs[...], (LANES, LANES + count)).T
        spread = column[LANES - HALO :]
        for lag in range(8, HALO, 8):
            same = spread[HALO - 8 :] == spread[HALO - 8 - lag : HALO + count - lag]
            far[lag // 8 - 1, pl.ds(HALO - 8, count + 8), :] = same.astype(jnp.float32)
        for lag in range(1, 8):
            same = spread[HALO:] == spread[HALO - lag : HALO + count - lag]
            near_by[lag - 1] = same.astype(jnp.float32)

    def project(block, part):
        held = weights[
            block, :, pl.ds(pl.multiple_of(part * 2 * LANES, 2 * LANES), 2 * LANES)
        ]
        both = jnp.dot(tok[...], held, preferred_element_type=jnp.float32)
        value = both[:, :LANES].astype(jnp.bfloat16).astype(jnp.float32)
        gate = both[:, LANES:].astype(jnp.bfloat16).astype(jnp.float32)
        glu = (value * jax.nn.sigmoid(gate)).astype(jnp.bfloat16).astype(jnp.float32)
        shifted[0] = glu

    def convolve(block, part):
        first = pl.multiple_of((block * parts + part) * LANES, LANES)
        lanes = pl.ds(first, LANES)
        kept = pl.ds(HALO - 8, count + 8)
        for a in range(1, HALO // 8):
            shifted[a, kept, :] = (
                shifted[0, pl.ds(HALO - 8 - 8 * a, count + 8), :] * far[a - 1, kept, :]
            )

        @pl.loop(0, count // TILE)
        def _(tile):
            top = pl.multiple_of(tile * TILE, TILE)
            total = None
            for r in range(8):
                run = None
                for a in range(HALO // 8):
                    lag = 8 * a + r
                    if lag < KERNEL:
                        moved = shifted[a, pl.ds(top + HALO - r, TILE), :]
                        term = moved * taps[lag : lag + 1, lanes]
                        run = term if run is None else run + term
                if r:
                    run = run * near_by[r - 1, pl.ds(top, TILE), :]
                total = run if total is None else total + run
            mixed_ref[pl.ds(top, TILE), lanes] = total.astype(jnp.bfloat16)

    def tick(at, carry):
        block, k = lax.div(at, tall), lax.rem(at, tall)

        @pl.when((block + AHEAD < blocks) & (k == 0))
        def _():
            send_own(block + AHEAD)

        @pl.when((block < blocks) & (k > 0))
        def _():
            arrived(block, near(k), u, v)

        second = jnp.maximum(at - second_start, 0)
        block2, k2 = lax.div(second, tall), lax.rem(second, tall)

        @pl.when((at >= second_start) & (block2 < blocks))
        def _():
            @pl.loop(1, side)
            def _(du):
                arrived(block2, near(k2), lax.rem(u + du, side), v)

        third = jnp.maximum(at - third_start, 0)
        block3, k3 = lax.div(third, tall), lax.rem(third, tall)

        @pl.when((at >= third_start) & (block3 < blocks))
        def _():
            @pl.loop(0, side)
            def _(du):
                @pl.loop(1, side)
                def _(dv):
                    arrived(block3, near(k3), lax.rem(u + du, side), lax.rem(v + dv, side))

        late = jnp.maximum(at - late_start, 0)
        block4, k4 = lax.div(late, tall), lax.rem(late, tall)

        @pl.when(at == second_start)
        def _():
            prepare()

        @pl.when((at >= late_start) & (k4 == 0))
        def _():
            @pl.loop(0, tall * side * side)
            def _(q):
                hand_over(1 - core, block4, q).wait_recv()

        part = lax.div(k4, 2)

        @pl.when((at >= late_start) & (lax.rem(k4, 2) == 0))
        def _():
            project(block4, part)

        @pl.when((at >= late_start) & (lax.rem(k4, 2) == 1))
        def _():
            convolve(block4, part)

        @pl.when(at >= late_start)
        def _():
            @pl.loop(0, side)
            def _(pu):
                @pl.loop(0, side)
                def _(pv):
                    routes(block4, k4, pu, pv, lambda copy: copy.wait_send())

        return carry

    lax.fori_loop(0, blocks * tall + late_start, tick, 0)

    @pl.when(sp + 1 < sp_size)
    def _():
        tail.wait_send()
        docs_tail.wait_send()


def mixed_product(rows, docs, value_weight, gate_weight, conv_weight):
    side = lax.axis_size("dp") // 2
    tall = lax.axis_size("sp") // side
    count, width = rows.shape
    channels = value_weight.shape[1]
    blocks = channels // (LANES * (tall // 2))
    pieces = tall * side * side
    return pl.pallas_call(
        functools.partial(fused_kernel, side, tall, blocks),
        out_shape=jax.ShapeDtypeStruct((count, channels), jnp.bfloat16),
        in_specs=[pl.BlockSpec(memory_space=pl.ANY)] * 4
        + [pl.BlockSpec(memory_space=pltpu.VMEM)],
        out_specs=pl.BlockSpec(memory_space=pltpu.VMEM),
        scratch_shapes=[
            pltpu.VMEM((blocks, width, LANES * tall), jnp.bfloat16),
            pltpu.VMEM((HALO + count, width), jnp.bfloat16),
            pltpu.VMEM((1, LANES + count), jnp.int32),
            pltpu.VMEM((HALO, channels), jnp.float32),
            pltpu.VMEM((HALO // 8, HALO + count, LANES), jnp.float32),
            pltpu.VMEM((HALO // 8 - 1, HALO + count, LANES), jnp.float32),
            pltpu.VMEM((7, count, LANES), jnp.float32),
            pltpu.SemaphoreType.DMA((7, KEPT, pieces)),
            pltpu.SemaphoreType.DMA((blocks, pieces)),
            pltpu.SemaphoreType.DMA((blocks, pieces)),
            pltpu.SemaphoreType.DMA((blocks, tall)),
            pltpu.SemaphoreType.DMA((2,)),
            pltpu.SemaphoreType.DMA((4,)),
        ],
        compiler_params=pltpu.CompilerParams(
            collective_id=0, has_side_effects=True, vmem_limit_bytes=56 * 1024 * 1024
        ),
    )(rows, docs, value_weight, gate_weight, conv_weight)


def norm_kernel(mixed_ref, gain_ref, bias_ref, out_ref):
    wide = mixed_ref[...].astype(jnp.float32)
    center = wide - jnp.mean(wide, axis=-1, keepdims=True)
    spread = jnp.mean(center * center, axis=-1, keepdims=True)
    normed = center * lax.rsqrt(spread + 1e-06) * gain_ref[...] + bias_ref[...]
    out_ref[...] = (normed * jax.nn.sigmoid(normed)).astype(jnp.bfloat16)


def finish(mixed, norm_gain, norm_bias):
    count, channels = mixed.shape
    rows = 64
    return pl.pallas_call(
        norm_kernel,
        grid=(count // rows,),
        out_shape=jax.ShapeDtypeStruct((count, channels), jnp.bfloat16),
        in_specs=[
            pl.BlockSpec((rows, channels), lambda i: (i, 0)),
            pl.BlockSpec((1, channels), lambda i: (0, 0)),
            pl.BlockSpec((1, channels), lambda i: (0, 0)),
        ],
        out_specs=pl.BlockSpec((rows, channels), lambda i: (i, 0)),
    )(mixed, norm_gain[None], norm_bias[None])


def per_device(tokens, documents, value_weight, gate_weight, conv_weight, norm_gain, norm_bias):
    batch, count, width = tokens.shape
    channels = value_weight.shape[1]
    rows = tokens.reshape(batch * count, width)
    mixed = mixed_product(rows, documents, value_weight, gate_weight, conv_weight)
    out = finish(mixed, norm_gain, norm_bias)
    return out.reshape(batch, count, channels)


def solution(mesh):
    return jax.shard_map(
        per_device,
        mesh=mesh,
        in_specs=(
            P("dp", "sp", None),
            P("dp", "sp"),
            P(("sp", "dp"), None),
            P(("sp", "dp"), None),
            P(),
            P(),
            P(),
        ),
        out_specs=P("dp", "sp", None),
        check_vma=False,
    )
```

time: 205 us -> 160 us (0.78)
  Pallas kernels: 188 us -> 159 us
  local copies, waits for them, and re-layouts: 6.77 us -> 0 us
  starting transfers between devices: 4.86 us -> 0 us
  other arithmetic: 4.25 us -> 0 us
    pallas_call x2, Pallas kernels: 188 us -> 159 us  [the longest x1 152 us: mixed_product(): pl.pallas_call(functools.partial(fused_kernel, side, tall, blocks), out_s...]
    reshape x5 -> x0, local copies, waits for them, and re-layouts: 5.15 us -> none  [the longest x2 2.48 us: gated_product(): value_weight.reshape(cut)]
    ppermute x1 -> x0, starting transfers between devices: 4.86 us -> none  [passed_along(): return lax.ppermute(block, axis, route)]
    transpose x1 -> x0, other arithmetic: 2.43 us -> none  [gated_product(): own.transpose(1, 2, 0, 3, 4, 5)]
  transfers between devices with their start and end apart: 1 -> 0, of which waited for: 0 -> 0; matrix products, arithmetic and copies ran while one was open for 5% -> 0% of each run, Pallas kernels for 79% -> 0%
where the time goes in v1:
time: 160 us; the launch traced here: 159 us
  Pallas kernels  159 us (99%)
    pallas_call x1, Pallas kernels, mixed_product(): pl.pallas_call(functools.partial(fused_kernel, side, tall, blocks), out_s...  152 us
    pallas_call x1, Pallas kernels, finish(): pl.pallas_call(norm_kernel, grid=(count // rows,), out_shape=jax.ShapeDty...  6.8 us

profile of v1, /device:TPU:0, one launch (start us, length us, event | category | flops | bytes accessed | tf_op | source)
XLA Modules:
  0.0 159.3 jit_solution(9587811990240416563)
XLA Ops:
  0.0 152.5 %shard_map.73.mixed_ref = bf16[512,2048]{1,0:T(8,128)(2,1)} custom-call(bf16[512,4096]{1,0:T(8,128)(2,1)} %bitcast.4, s32[1,512]{1,0:T(1,128)} %docs_hbm.1, bf16[128,2048]{1,0:T(8,128)(2,1)} %value_hbm.1, bf16[128,2048]{1,0:T(8,128)(2,1)} %gate_hbm.1, bf16[31,2048]{1,0:T(8,128)(2,1)} %conv_ref.1), custom_call_target="tpu_custom_call" | custom-call | tf_op jit(solution)/shard_map/pallas_call | solution.py:320
  152.5 6.8 %shard_map.74 = bf16[512,2048]{1,0:T(8,128)(2,1)} custom-call(bf16[512,2048]{1,0:T(8,128)(2,1)} %shard_map.73.mixed_ref, f32[1,2048]{1,0:T(1,128)} %bitcast.5, f32[1,2048]{1,0:T(1,128)} %bitcast.6), custom_call_target="tpu_custom_call" | custom-call | tf_op jit(solution)/shard_map/pallas_call | solution.py:358

commit v2 on v1

--- a/solution.py
+++ b/solution.py
@@ -11,13 +11,27 @@
 HALO = 32
 LANES = 128
 TILE = 64
-AHEAD = 1
-KEPT = 5
 MESH = pl.DeviceIdType.MESH
 
 
+def plan(side, tall, channels):
+    order = dict(blocks=channels // LANES, tall_first=(0, 2, 6, 7, 11, 12), own=52)
+    if side == 2 and tall == 4:
+        order.update(along_z=(2, 4, 6), along_u=(0, 6, 9, 9), near_v=(17, 15, 12, 16), far_v=(12, 16, 17, 18), late=20)
+    else:
+        order.update(
+            own=tall,
+            along_z=tuple(range(1, tall)),
+            along_u=tuple(range(2, tall + 2)),
+            near_v=tuple(range(6, tall + 6)),
+            far_v=tuple(range(6, tall + 6)),
+            late=6 + tall,
+        )
+    return order
+
+
 def fused_kernel(
-    side, tall, blocks, tok_hbm, docs_hbm, value_hbm, gate_hbm, conv_ref, mixed_ref,
+    side, tall, order, tok_hbm, docs_hbm, value_hbm, gate_hbm, conv_ref, mixed_ref,
     weights, tok, docs, taps, shifted, far, near_by, send, recv, cross, own, begin, halo
 ):
     sp, dp = lax.axis_index("sp"), lax.axis_index("dp")
@@ -28,11 +42,12 @@
     u, v = jnp.where(flip, y, x), jnp.where(flip, x, y)
     depth = value_hbm.shape[0]
     count = tok_hbm.shape[0]
-    parts = tall // 2
-    second_start, third_start = 2, 6
-    late_start = third_start + tall
+    blocks = order["blocks"]
+    parts = mixed_ref.shape[1] // (blocks * LANES)
     other = {"sp": sp, "dp": y * 2 + (1 - core)}
     here = (z * side + x) * side + y
+
+    pieces = tall * side * side
 
     def device(dz, du, dv):
         dx, dy = jnp.where(flip, dv, du), jnp.where(flip, du, dv)
@@ -51,46 +66,97 @@
         return pltpu.make_async_remote_copy(
             src_ref=piece(core, block, q),
             dst_ref=piece(core, block, q),
-            send_sem=send.at[kind, lax.rem(block, KEPT), q],
+            send_sem=send.at[kind, block],
             recv_sem=recv.at[block, q],
             device_id=target,
             device_id_type=MESH,
         )
 
-    def hand_over(which, block, q):
+    def hand_over(rows, block):
         return pltpu.make_async_remote_copy(
-            src_ref=piece(which, block, q),
-            dst_ref=piece(which, block, q),
-            send_sem=send.at[6, lax.rem(block, KEPT), q],
-            recv_sem=cross.at[block, q],
+            src_ref=rows,
+            dst_ref=rows,
+            send_sem=send.at[6, block],
+            recv_sem=cross.at[block],
             device_id=other,
             device_id_type=MESH,
         )
 
-    def routes(block, pz, pu, pv, act):
+    def many(block, amount):
+        return weights.at[block, pl.ds(0, amount * depth), :]
+
+    def tall_first(block):
+        return functools.reduce(
+            jnp.logical_or, [block == chosen for chosen in order["tall_first"]]
+        )
+
+    def spread(kind, block, q, at, source, extent, target, allowed):
+        if source is at:
+            if extent == 2:
+                ways = (((None), 1 - at, kind),)
+            else:
+                ways = ((at + 1 < extent, at + 1, kind), (at > 0, at - 1, kind + 1))
+        elif extent == 2:
+            return
+        else:
+            rising = at > source
+            onward = jnp.where(rising, at + 1, at - 1)
+            inside = (onward >= 0) & (onward < extent)
+            ways = ((inside, onward, jnp.where(rising, kind, kind + 1)),)
+        for taken, onward, which in ways:
+            conditions = [c for c in (taken, allowed) if c is not None]
+            copy = link(which, block, q, target(onward))
+            if conditions:
+                pl.when(functools.reduce(jnp.logical_and, conditions))(copy.start)
+            else:
+                copy.start()
+
+    def pass_on(block, pz, pu, pv):
         q = number(pz, pu, pv)
-        tall_first = (block == 1) | (block == 4) | (block == 6)
-        home_u, home_v, home_z = u == pu, v == pv, z == pz
-        along_z = home_v & (home_u | jnp.logical_not(tall_first))
-        along_u = home_v & (home_z | tall_first)
-        ways = (
-            (along_z & (z >= pz) & (z + 1 < tall), (z + 1, u, v)),
-            (along_z & (z <= pz) & (z > 0), (z - 1, u, v)),
-            (along_u & (u >= pu) & (u + 1 < side), (z, u + 1, v)),
-            (along_u & (u <= pu) & (u > 0), (z, u - 1, v)),
-            ((v >= pv) & (v + 1 < side), (z, u, v + 1)),
-            ((v <= pv) & (v > 0), (z, u, v - 1)),
-        )
-        for kind, (taken, target) in enumerate(ways):
-
-            @pl.when(taken)
-            def _(kind=kind, target=target):
-                act(link(kind, block, q, device(*target)))
-
-        act(hand_over(core, block, q))
-
-    def pass_on(block, pz, pu, pv):
-        routes(block, pz, pu, pv, lambda copy: copy.start())
+        first = tall_first(block)
+        if pv is v:
+            along_z = None if pu is u else jnp.logical_not(first)
+            spread(0, block, q, z, pz, tall, lambda to: device(to, u, v), along_z)
+            along_u = None if pz is z else first
+            spread(2, block, q, u, pu, side, lambda to: device(z, to, v), along_u)
+        spread(4, block, q, v, pv, side, lambda to: device(z, u, to), None)
+        hand_over(piece(core, block, q), block).start()
+
+    def sent(kind, block, amount, choices):
+        for chosen in choices:
+            copy = pltpu.make_async_remote_copy(
+                src_ref=many(block, chosen),
+                dst_ref=many(block, chosen),
+                send_sem=send.at[kind, block],
+                recv_sem=cross.at[block],
+                device_id=other,
+                device_id_type=MESH,
+            )
+            pl.when(amount == chosen)(copy.wait_send)
+
+    def all_sent(block):
+        first = tall_first(block)
+        across = jnp.where(first, 1, side)
+        up = jnp.where(z + 1 < tall, (z + 1) * across, 0)
+        down = jnp.where(z > 0, (tall - z) * across, 0)
+        choices = sorted({n * m for n in range(1, tall + 1) for m in (1, side)})
+        sent(0, block, up, choices)
+        sent(1, block, down, choices)
+        height = jnp.where(first, tall, 1)
+        if side == 2:
+            sent(2, block, height, (1, tall))
+        else:
+            choices = sorted({n * m for n in range(1, side + 1) for m in (1, tall)})
+            sent(2, block, jnp.where(u + 1 < side, (u + 1) * height, 0), choices)
+            sent(3, block, jnp.where(u > 0, (side - u) * height, 0), choices)
+        plane = tall * side
+        if side == 2:
+            sent(4, block, jnp.int32(plane), (plane,))
+        else:
+            choices = [n * plane for n in range(1, side + 1)]
+            sent(4, block, jnp.where(v + 1 < side, (v + 1) * plane, 0), choices)
+            sent(5, block, jnp.where(v > 0, (side - v) * plane, 0), choices)
+        hand_over(many(block, pieces), block).wait_send()
 
     def arrived(block, pz, pu, pv):
         link(0, block, number(pz, pu, pv), other).wait_recv()
@@ -168,7 +234,9 @@
         device_id_type=MESH,
     )
 
-    @pl.loop(0, AHEAD)
+    ahead = min(blocks, -(-order["own"] // tall))
+
+    @pl.loop(0, ahead)
     def _(block):
         send_own(block)
 
@@ -194,12 +262,12 @@
             docs_tail.wait_recv()
 
         column = jnp.broadcast_to(docs[...], (LANES, LANES + count)).T
-        spread = column[LANES - HALO :]
+        wide = column[LANES - HALO :]
         for lag in range(8, HALO, 8):
-            same = spread[HALO - 8 :] == spread[HALO - 8 - lag : HALO + count - lag]
+            same = wide[HALO - 8 :] == wide[HALO - 8 - lag : HALO + count - lag]
             far[lag // 8 - 1, pl.ds(HALO - 8, count + 8), :] = same.astype(jnp.float32)
         for lag in range(1, 8):
-            same = spread[HALO:] == spread[HALO - lag : HALO + count - lag]
+            same = wide[HALO:] == wide[HALO - lag : HALO + count - lag]
             near_by[lag - 1] = same.astype(jnp.float32)
 
     def project(block, part):
@@ -238,71 +306,66 @@
                 total = run if total is None else total + run
             mixed_ref[pl.ds(top, TILE), lanes] = total.astype(jnp.bfloat16)
 
-    def tick(at, carry):
-        block, k = lax.div(at, tall), lax.rem(at, tall)
-
-        @pl.when((block + AHEAD < blocks) & (k == 0))
-        def _():
-            send_own(block + AHEAD)
-
-        @pl.when((block < blocks) & (k > 0))
-        def _():
-            arrived(block, near(k), u, v)
-
-        second = jnp.maximum(at - second_start, 0)
-        block2, k2 = lax.div(second, tall), lax.rem(second, tall)
-
-        @pl.when((at >= second_start) & (block2 < blocks))
-        def _():
+    def level(k):
+        return z if k == 0 else near(k)
+
+    def near_u(block, k):
+        @pl.loop(1, side)
+        def _(du):
+            arrived(block, level(k), lax.rem(u + du, side), v)
+
+    def near_v(block, k):
+        @pl.loop(1, side)
+        def _(dv):
+            arrived(block, level(k), u, lax.rem(v + dv, side))
+
+    def far_v(block, k):
+        @pl.loop(1, side)
+        def _(du):
             @pl.loop(1, side)
-            def _(du):
-                arrived(block2, near(k2), lax.rem(u + du, side), v)
-
-        third = jnp.maximum(at - third_start, 0)
-        block3, k3 = lax.div(third, tall), lax.rem(third, tall)
-
-        @pl.when((at >= third_start) & (block3 < blocks))
-        def _():
-            @pl.loop(0, side)
-            def _(du):
-                @pl.loop(1, side)
-                def _(dv):
-                    arrived(block3, near(k3), lax.rem(u + du, side), lax.rem(v + dv, side))
-
-        late = jnp.maximum(at - late_start, 0)
-        block4, k4 = lax.div(late, tall), lax.rem(late, tall)
-
-        @pl.when(at == second_start)
-        def _():
-            prepare()
-
-        @pl.when((at >= late_start) & (k4 == 0))
-        def _():
-            @pl.loop(0, tall * side * side)
-            def _(q):
-                hand_over(1 - core, block4, q).wait_recv()
-
-        part = lax.div(k4, 2)
-
-        @pl.when((at >= late_start) & (lax.rem(k4, 2) == 0))
-        def _():
-            project(block4, part)
-
-        @pl.when((at >= late_start) & (lax.rem(k4, 2) == 1))
-        def _():
-            convolve(block4, part)
-
-        @pl.when(at >= late_start)
-        def _():
-            @pl.loop(0, side)
-            def _(pu):
-                @pl.loop(0, side)
-                def _(pv):
-                    routes(block4, k4, pu, pv, lambda copy: copy.wait_send())
+            def _(dv):
+                arrived(block, level(k), lax.rem(u + du, side), lax.rem(v + dv, side))
+
+    def compute(block, k):
+        if k == 0:
+            hand_over(many(block, pieces), block).wait_recv()
+
+        for step in range(k * 2 * parts // tall, (k + 1) * 2 * parts // tall):
+            if step % 2 == 0:
+                project(block, step // 2)
+            else:
+                convolve(block, step // 2)
+
+        if k == tall - 1:
+            all_sent(block)
+
+    sites = [(-order["own"], lambda block: send_own(block))]
+    for k in range(1, tall):
+        sites.append((order["along_z"][k - 1], lambda block, k=k: arrived(block, near(k), u, v)))
+    for name, act in (("along_u", near_u), ("near_v", near_v), ("far_v", far_v)):
+        for k in range(tall):
+            sites.append((order[name][k], lambda block, k=k, act=act: act(block, k)))
+    for k in range(tall):
+        sites.append((order["late"] + k, lambda block, k=k: compute(block, k)))
+    assert all(offset <= order["late"] for offset, _ in sites[:-tall])
+
+    def round_of(number, carry):
+        for j in range(tall):
+            for offset, act in sites:
+                if offset % tall != j:
+                    continue
+                block = number - offset // tall
+                first = ahead if offset < 0 else 0
+
+                @pl.when((block >= first) & (block < blocks))
+                def _(block=block, act=act):
+                    act(block)
 
         return carry
 
-    lax.fori_loop(0, blocks * tall + late_start, tick, 0)
+    prepare()
+    rounds = blocks + (order["late"] + tall - 1) // tall
+    lax.fori_loop(0, rounds, round_of, 0)
 
     @pl.when(sp + 1 < sp_size)
     def _():
@@ -315,26 +378,27 @@
     tall = lax.axis_size("sp") // side
     count, width = rows.shape
     channels = value_weight.shape[1]
-    blocks = channels // (LANES * (tall // 2))
+    order = plan(side, tall, channels)
+    blocks = order["blocks"]
     pieces = tall * side * side
     return pl.pallas_call(
-        functools.partial(fused_kernel, side, tall, blocks),
+        functools.partial(fused_kernel, side, tall, order),
         out_shape=jax.ShapeDtypeStruct((count, channels), jnp.bfloat16),
         in_specs=[pl.BlockSpec(memory_space=pl.ANY)] * 4
         + [pl.BlockSpec(memory_space=pltpu.VMEM)],
         out_specs=pl.BlockSpec(memory_space=pltpu.VMEM),
         scratch_shapes=[
-            pltpu.VMEM((blocks, width, LANES * tall), jnp.bfloat16),
+            pltpu.VMEM((blocks, width, 2 * channels // blocks), jnp.bfloat16),
             pltpu.VMEM((HALO + count, width), jnp.bfloat16),
             pltpu.VMEM((1, LANES + count), jnp.int32),
             pltpu.VMEM((HALO, channels), jnp.float32),
             pltpu.VMEM((HALO // 8, HALO + count, LANES), jnp.float32),
             pltpu.VMEM((HALO // 8 - 1, HALO + count, LANES), jnp.float32),
             pltpu.VMEM((7, count, LANES), jnp.float32),
-            pltpu.SemaphoreType.DMA((7, KEPT, pieces)),
+            pltpu.SemaphoreType.DMA((7, blocks)),
             pltpu.SemaphoreType.DMA((blocks, pieces)),
-            pltpu.SemaphoreType.DMA((blocks, pieces)),
-            pltpu.SemaphoreType.DMA((blocks, tall)),
+            pltpu.SemaphoreType.DMA((blocks,)),
+            pltpu.SemaphoreType.DMA((blocks, 2 * channels // (blocks * LANES))),
             pltpu.SemaphoreType.DMA((2,)),
             pltpu.SemaphoreType.DMA((4,)),
         ],

time: 160 us -> 149 us (0.931)
  Pallas kernels: 159 us -> 149 us
    pallas_call x1, Pallas kernels: 152 us -> 142 us  [mixed_product(): pl.pallas_call(functools.partial(fused_kernel, side, tall, order), out_sh...]
where the time goes in v2:
time: 149 us
  Pallas kernels  149 us (100%)
    pallas_call x1, Pallas kernels, mixed_product(): pl.pallas_call(functools.partial(fused_kernel, side, tall, order), out_sh...  142 us
    pallas_call x1, Pallas kernels, finish(): pl.pallas_call(norm_kernel, grid=(count // rows,), out_shape=jax.ShapeDty...  6.8 us

profile of v2, /device:TPU:0, one launch (start us, length us, event | category | flops | bytes accessed | tf_op | source)
XLA Modules:
  0.0 148.6 jit_solution(9432774525256418988)
XLA Ops:
  0.0 141.8 %shard_map.73.mixed_ref = bf16[512,2048]{1,0:T(8,128)(2,1)} custom-call(bf16[512,4096]{1,0:T(8,128)(2,1)} %bitcast.4, s32[1,512]{1,0:T(1,128)} %docs_hbm.1, bf16[128,2048]{1,0:T(8,128)(2,1)} %value_hbm.1, bf16[128,2048]{1,0:T(8,128)(2,1)} %gate_hbm.1, bf16[31,2048]{1,0:T(8,128)(2,1)} %conv_ref.1), custom_call_target="tpu_custom_call" | custom-call | tf_op jit(solution)/shard_map/pallas_call | solution.py:384
  141.8 6.8 %shard_map.74 = bf16[512,2048]{1,0:T(8,128)(2,1)} custom-call(bf16[512,2048]{1,0:T(8,128)(2,1)} %shard_map.73.mixed_ref, f32[1,2048]{1,0:T(1,128)} %bitcast.5, f32[1,2048]{1,0:T(1,128)} %bitcast.6), custom_call_target="tpu_custom_call" | custom-call | tf_op jit(solution)/shard_map/pallas_call | solution.py:422

commit v3 on v2

--- a/solution.py
+++ b/solution.py
@@ -10,14 +10,16 @@
 KERNEL = 31
 HALO = 32
 LANES = 128
-TILE = 64
+TILE = 128
+SPARE = 8
+LEAVE = 32
 MESH = pl.DeviceIdType.MESH
 
 
 def plan(side, tall, channels):
-    order = dict(blocks=channels // LANES, tall_first=(0, 2, 6, 7, 11, 12), own=52)
+    order = dict(blocks=channels // LANES, tall_first=(1, 4, 7, 10, 13), own=20)
     if side == 2 and tall == 4:
-        order.update(along_z=(2, 4, 6), along_u=(0, 6, 9, 9), near_v=(17, 15, 12, 16), far_v=(12, 16, 17, 18), late=20)
+        order.update(along_z=(0, 4, 7), along_u=(0, 7, 8, 10), near_v=(3, 9, 11, 11), far_v=(9, 13, 13, 13), late=15)
     else:
         order.update(
             own=tall,
@@ -31,8 +33,9 @@
 
 
 def fused_kernel(
-    side, tall, order, tok_hbm, docs_hbm, value_hbm, gate_hbm, conv_ref, mixed_ref,
-    weights, tok, docs, taps, shifted, far, near_by, send, recv, cross, own, begin, halo
+    side, tall, order, tok_hbm, docs_hbm, value_hbm, gate_hbm, conv_ref, gain_ref,
+    bias_ref, out_hbm, weights, tok, docs, taps, shifted, far, near_by, mixed, center,
+    total, square, send, recv, cross, own, begin, halo, leave
 ):
     sp, dp = lax.axis_index("sp"), lax.axis_index("dp")
     sp_size = lax.axis_size("sp")
@@ -43,7 +46,9 @@
     depth = value_hbm.shape[0]
     count = tok_hbm.shape[0]
     blocks = order["blocks"]
-    parts = mixed_ref.shape[1] // (blocks * LANES)
+    channels = value_hbm.shape[1]
+    parts = channels // (blocks * LANES)
+    lines = (HALO + count) // 2
     other = {"sp": sp, "dp": y * 2 + (1 - core)}
     here = (z * side + x) * side + y
 
@@ -185,16 +190,6 @@
             copy.wait()
         pass_on(block, z, u, v)
 
-    @pl.loop(0, blocks)
-    def _(block):
-        for copy in own_copies(block):
-            copy.start()
-
-    load = pltpu.make_async_copy(tok_hbm, tok.at[pl.ds(HALO, count), :], begin.at[0])
-    load.start()
-    read = pltpu.make_async_copy(docs_hbm, docs.at[:, pl.ds(LANES, count)], begin.at[1])
-    read.start()
-
     barrier = pltpu.get_barrier_semaphore()
     greeted = jnp.int32(1)
     pl.semaphore_signal(barrier, inc=1, device_id=other, device_id_type=MESH)
@@ -213,6 +208,16 @@
         @pl.when(there)
         def _(target=target):
             pl.semaphore_signal(barrier, inc=1, device_id=target, device_id_type=MESH)
+
+    @pl.loop(0, blocks)
+    def _(block):
+        for copy in own_copies(block):
+            copy.start()
+
+    load = pltpu.make_async_copy(tok_hbm, tok.at[pl.ds(HALO, count), :], begin.at[0])
+    load.start()
+    read = pltpu.make_async_copy(docs_hbm, docs.at[:, pl.ds(LANES, count)], begin.at[1])
+    read.start()
 
     pl.semaphore_wait(barrier, greeted)
 
@@ -234,16 +239,16 @@
         device_id_type=MESH,
     )
 
-    ahead = min(blocks, -(-order["own"] // tall))
-
-    @pl.loop(0, ahead)
-    def _(block):
-        send_own(block)
-
     @pl.when(sp + 1 < sp_size)
     def _():
         tail.start()
         docs_tail.start()
+
+    ahead = min(blocks, -(-order["own"] // tall))
+
+    @pl.loop(0, ahead)
+    def _(block):
+        send_own(block)
 
     @pl.when(sp == 0)
     def _():
@@ -268,31 +273,36 @@
             far[lag // 8 - 1, pl.ds(HALO - 8, count + 8), :] = same.astype(jnp.float32)
         for lag in range(1, 8):
             same = wide[HALO:] == wide[HALO - lag : HALO + count - lag]
-            near_by[lag - 1] = same.astype(jnp.float32)
-
-    def project(block, part):
+            near_by[lag - 1, pl.ds(0, count), :] = same.astype(jnp.float32)
+
+        total[...] = jnp.zeros_like(total)
+        square[...] = jnp.zeros_like(square)
+
+    def project(block, part, half):
+        rows = pl.ds(half * lines, lines)
         held = weights[
             block, :, pl.ds(pl.multiple_of(part * 2 * LANES, 2 * LANES), 2 * LANES)
         ]
-        both = jnp.dot(tok[...], held, preferred_element_type=jnp.float32)
+        both = jnp.dot(tok[rows, :], held, preferred_element_type=jnp.float32)
         value = both[:, :LANES].astype(jnp.bfloat16).astype(jnp.float32)
         gate = both[:, LANES:].astype(jnp.bfloat16).astype(jnp.float32)
         glu = (value * jax.nn.sigmoid(gate)).astype(jnp.bfloat16).astype(jnp.float32)
-        shifted[0] = glu
-
-    def convolve(block, part):
+        shifted[0, rows, :] = glu
+
+    def convolve(block, part, half):
         first = pl.multiple_of((block * parts + part) * LANES, LANES)
         lanes = pl.ds(first, LANES)
-        kept = pl.ds(HALO - 8, count + 8)
+        span = count // 2
+        start = half * span + HALO - 8
+        kept = pl.ds(start, span + 8)
         for a in range(1, HALO // 8):
-            shifted[a, kept, :] = (
-                shifted[0, pl.ds(HALO - 8 - 8 * a, count + 8), :] * far[a - 1, kept, :]
-            )
-
-        @pl.loop(0, count // TILE)
+            moved = shifted[0, pl.ds(start - 8 * a, span + 8), :]
+            shifted[a, kept, :] = moved * far[a - 1, kept, :]
+
+        @pl.loop(0, span // TILE)
         def _(tile):
-            top = pl.multiple_of(tile * TILE, TILE)
-            total = None
+            top = pl.multiple_of(half * span + tile * TILE, TILE)
+            held = None
             for r in range(8):
                 run = None
                 for a in range(HALO // 8):
@@ -303,8 +313,46 @@
                         run = term if run is None else run + term
                 if r:
                     run = run * near_by[r - 1, pl.ds(top, TILE), :]
-                total = run if total is None else total + run
-            mixed_ref[pl.ds(top, TILE), lanes] = total.astype(jnp.bfloat16)
+                held = run if held is None else held + run
+            rows = pl.ds(top, TILE)
+            rounded = held.astype(jnp.bfloat16)
+            mixed[rows, lanes] = rounded
+            held = rounded.astype(jnp.float32)
+
+            @pl.when(first == 0)
+            def _():
+                middle = jnp.mean(held, axis=-1, keepdims=True)
+                center[rows, :] = jnp.broadcast_to(middle, (TILE, LANES))
+
+            off = held - center[rows, :]
+            total[rows, :] += off
+            square[rows, :] += off * off
+
+    def leaving(step):
+        rows = pl.ds(pl.multiple_of(step * LEAVE, LEAVE), LEAVE)
+        return pltpu.make_async_copy(mixed.at[rows, :], out_hbm.at[rows, :], leave.at[step])
+
+    def finish():
+        moved = jnp.sum(total[...], axis=-1, keepdims=True) / channels
+        spread = jnp.sum(square[...], axis=-1, keepdims=True) / channels - moved * moved
+        scale = lax.rsqrt(jnp.maximum(spread, 0.0) + 1e-06)
+        center[...] = center[...] + moved
+        total[...] = jnp.broadcast_to(scale, total.shape)
+
+        @pl.loop(0, count // LEAVE)
+        def _(step):
+            rows = pl.ds(pl.multiple_of(step * LEAVE, LEAVE), LEAVE)
+            middle, scale = center[rows, :], total[rows, :]
+            for lane in range(0, channels, LANES):
+                lanes = pl.ds(lane, LANES)
+                wide = mixed[rows, lanes].astype(jnp.float32)
+                normed = (wide - middle) * scale * gain_ref[:, lanes] + bias_ref[:, lanes]
+                mixed[rows, lanes] = (normed * jax.nn.sigmoid(normed)).astype(jnp.bfloat16)
+            leaving(step).start()
+
+        @pl.loop(0, count // LEAVE)
+        def _(step):
+            leaving(step).wait()
 
     def level(k):
         return z if k == 0 else near(k)
@@ -328,13 +376,17 @@
 
     def compute(block, k):
         if k == 0:
+            pl.when(block == 0)(prepare)
             hand_over(many(block, pieces), block).wait_recv()
 
-        for step in range(k * 2 * parts // tall, (k + 1) * 2 * parts // tall):
-            if step % 2 == 0:
-                project(block, step // 2)
-            else:
-                convolve(block, step // 2)
+        steps = [
+            (act, part, half)
+            for part in range(parts)
+            for act in (project, convolve)
+            for half in range(2)
+        ]
+        for act, part, half in steps[k * len(steps) // tall : (k + 1) * len(steps) // tall]:
+            act(block, part, half)
 
         if k == tall - 1:
             all_sent(block)
@@ -363,9 +415,9 @@
 
         return carry
 
-    prepare()
     rounds = blocks + (order["late"] + tall - 1) // tall
     lax.fori_loop(0, rounds, round_of, 0)
+    finish()
 
     @pl.when(sp + 1 < sp_size)
     def _():
@@ -373,7 +425,9 @@
         docs_tail.wait_send()
 
 
-def mixed_product(rows, docs, value_weight, gate_weight, conv_weight):
+def activated_product(
+    rows, docs, value_weight, gate_weight, conv_weight, norm_gain, norm_bias
+):
     side = lax.axis_size("dp") // 2
     tall = lax.axis_size("sp") // side
     count, width = rows.shape
@@ -385,59 +439,43 @@
         functools.partial(fused_kernel, side, tall, order),
         out_shape=jax.ShapeDtypeStruct((count, channels), jnp.bfloat16),
         in_specs=[pl.BlockSpec(memory_space=pl.ANY)] * 4
-        + [pl.BlockSpec(memory_space=pltpu.VMEM)],
-        out_specs=pl.BlockSpec(memory_space=pltpu.VMEM),
+        + [pl.BlockSpec(memory_space=pltpu.VMEM)] * 3,
+        out_specs=pl.BlockSpec(memory_space=pl.ANY),
         scratch_shapes=[
             pltpu.VMEM((blocks, width, 2 * channels // blocks), jnp.bfloat16),
             pltpu.VMEM((HALO + count, width), jnp.bfloat16),
             pltpu.VMEM((1, LANES + count), jnp.int32),
             pltpu.VMEM((HALO, channels), jnp.float32),
-            pltpu.VMEM((HALO // 8, HALO + count, LANES), jnp.float32),
-            pltpu.VMEM((HALO // 8 - 1, HALO + count, LANES), jnp.float32),
-            pltpu.VMEM((7, count, LANES), jnp.float32),
+            pltpu.VMEM((HALO // 8, HALO + count + SPARE, LANES), jnp.float32),
+            pltpu.VMEM((HALO // 8 - 1, HALO + count + SPARE, LANES), jnp.float32),
+            pltpu.VMEM((7, count + SPARE, LANES), jnp.float32),
+            pltpu.VMEM((count, channels), jnp.bfloat16),
+            pltpu.VMEM((count, LANES), jnp.float32),
+            pltpu.VMEM((count, LANES), jnp.float32),
+            pltpu.VMEM((count, LANES), jnp.float32),
             pltpu.SemaphoreType.DMA((7, blocks)),
             pltpu.SemaphoreType.DMA((blocks, pieces)),
             pltpu.SemaphoreType.DMA((blocks,)),
             pltpu.SemaphoreType.DMA((blocks, 2 * channels // (blocks * LANES))),
             pltpu.SemaphoreType.DMA((2,)),
             pltpu.SemaphoreType.DMA((4,)),
+            pltpu.SemaphoreType.DMA((count // LEAVE,)),
         ],
         compiler_params=pltpu.CompilerParams(
             collective_id=0, has_side_effects=True, vmem_limit_bytes=56 * 1024 * 1024
         ),
-    )(rows, docs, value_weight, gate_weight, conv_weight)
-
-
-def norm_kernel(mixed_ref, gain_ref, bias_ref, out_ref):
-    wide = mixed_ref[...].astype(jnp.float32)
-    center = wide - jnp.mean(wide, axis=-1, keepdims=True)
-    spread = jnp.mean(center * center, axis=-1, keepdims=True)
-    normed = center * lax.rsqrt(spread + 1e-06) * gain_ref[...] + bias_ref[...]
-    out_ref[...] = (normed * jax.nn.sigmoid(normed)).astype(jnp.bfloat16)
-
-
-def finish(mixed, norm_gain, norm_bias):
-    count, channels = mixed.shape
-    rows = 64
-    return pl.pallas_call(
-        norm_kernel,
-        grid=(count // rows,),
-        out_shape=jax.ShapeDtypeStruct((count, channels), jnp.bfloat16),
-        in_specs=[
-            pl.BlockSpec((rows, channels), lambda i: (i, 0)),
-            pl.BlockSpec((1, channels), lambda i: (0, 0)),
-            pl.BlockSpec((1, channels), lambda i: (0, 0)),
-        ],
-        out_specs=pl.BlockSpec((rows, channels), lambda i: (i, 0)),
-    )(mixed, norm_gain[None], norm_bias[None])
+    )(
+        rows, docs, value_weight, gate_weight, conv_weight, norm_gain[None], norm_bias[None]
+    )
 
 
 def per_device(tokens, documents, value_weight, gate_weight, conv_weight, norm_gain, norm_bias):
     batch, count, width = tokens.shape
     channels = value_weight.shape[1]
     rows = tokens.reshape(batch * count, width)
-    mixed = mixed_product(rows, documents, value_weight, gate_weight, conv_weight)
-    out = finish(mixed, norm_gain, norm_bias)
+    out = activated_product(
+        rows, documents, value_weight, gate_weight, conv_weight, norm_gain, norm_bias
+    )
     return out.reshape(batch, count, channels)
 
 

time: 149 us -> 142 us (0.953)
  Pallas kernels: 149 us -> 139 us
  local copies, waits for them, and re-layouts: 0 us -> 3.16 us
    pallas_call x2 -> x1, Pallas kernels: 149 us -> 139 us  [activated_product(): pl.pallas_call(functools.partial(fused_kernel, side, tall, order), out_sh...]
    unnamed x0 -> x1, local copies, waits for them, and re-layouts: none -> 3.16 us
where the time goes in v3:
time: 142 us
  Pallas kernels  139 us (98%)
  local copies, waits for them, and re-layouts  3.16 us (2%)
    pallas_call x1, Pallas kernels, activated_product(): pl.pallas_call(functools.partial(fused_kernel, side, tall, order), out_sh...  139 us
    unnamed x1, local copies, waits for them, and re-layouts  3.16 us

profile of v3, /device:TPU:0, one launch (start us, length us, event | category | flops | bytes accessed | tf_op | source)
XLA Modules:
  0.0 142.0 jit_solution(17233836824707291104)
XLA Ops:
  0.0 138.8 %shard_map.73 = bf16[512,2048]{1,0:T(8,128)(2,1)} custom-call(bf16[512,4096]{1,0:T(8,128)(2,1)} %bitcast.5, s32[1,512]{1,0:T(1,128)} %docs_hbm.1, bf16[128,2048]{1,0:T(8,128)(2,1)} %value_hbm.1, bf16[128,2048]{1,0:T(8,128)(2,1)} %gate_hbm.1, bf16[31,2048]{1,0:T(8,128)(2,1)} %conv_ref.1, f32[1,2048]{1,0:T(1,128)} %bitcast.6, f32[1,2048]{1,0:T(1,128)} %bitcast.7), custom_call_target="tpu_custom_call" | custom-call | tf_op jit(solution)/shard_map/pallas_call | solution.py:438
  138.8 3.2 %copy.9 = bf16[1,512,2048]{2,1,0:T(8,128)(2,1)} copy(bf16[1,512,2048]{2,1,0:T(8,128)(2,1)} %bitcast.4) | data formatting | bytes 4194304

commit v4 on v3

--- a/solution.py
+++ b/solution.py
@@ -17,9 +17,9 @@
 
 
 def plan(side, tall, channels):
-    order = dict(blocks=channels // LANES, tall_first=(1, 4, 7, 10, 13), own=20)
+    order = dict(blocks=channels // LANES, tall_first=((1, 4, 7, 10, 13), (0, 2, 7, 8, 11, 13)), own=47)
     if side == 2 and tall == 4:
-        order.update(along_z=(0, 4, 7), along_u=(0, 7, 8, 10), near_v=(3, 9, 11, 11), far_v=(9, 13, 13, 13), late=15)
+        order.update(along_z=(0, 4, 7), along_u=(0, 7, 9, 10), near_v=(5, 11, 12, 12), far_v=(9, 13, 14, 14), late=16)
     else:
         order.update(
             own=tall,
@@ -34,8 +34,8 @@
 
 def fused_kernel(
     side, tall, order, tok_hbm, docs_hbm, value_hbm, gate_hbm, conv_ref, gain_ref,
-    bias_ref, out_hbm, weights, tok, docs, taps, shifted, far, near_by, mixed, center,
-    total, square, send, recv, cross, own, begin, halo, leave
+    bias_ref, mixed, weights, tok, docs, taps, shifted, far, near_by, center,
+    total, square, send, recv, cross, own, begin, halo
 ):
     sp, dp = lax.axis_index("sp"), lax.axis_index("dp")
     sp_size = lax.axis_size("sp")
@@ -92,7 +92,12 @@
 
     def tall_first(block):
         return functools.reduce(
-            jnp.logical_or, [block == chosen for chosen in order["tall_first"]]
+            jnp.logical_or,
+            [
+                (core == which) & (block == chosen)
+                for which in range(2)
+                for chosen in order["tall_first"][which]
+            ],
         )
 
     def spread(kind, block, q, at, source, extent, target, allowed):
@@ -328,10 +333,6 @@
             total[rows, :] += off
             square[rows, :] += off * off
 
-    def leaving(step):
-        rows = pl.ds(pl.multiple_of(step * LEAVE, LEAVE), LEAVE)
-        return pltpu.make_async_copy(mixed.at[rows, :], out_hbm.at[rows, :], leave.at[step])
-
     def finish():
         moved = jnp.sum(total[...], axis=-1, keepdims=True) / channels
         spread = jnp.sum(square[...], axis=-1, keepdims=True) / channels - moved * moved
@@ -348,11 +349,6 @@
                 wide = mixed[rows, lanes].astype(jnp.float32)
                 normed = (wide - middle) * scale * gain_ref[:, lanes] + bias_ref[:, lanes]
                 mixed[rows, lanes] = (normed * jax.nn.sigmoid(normed)).astype(jnp.bfloat16)
-            leaving(step).start()
-
-        @pl.loop(0, count // LEAVE)
-        def _(step):
-            leaving(step).wait()
 
     def level(k):
         return z if k == 0 else near(k)
@@ -437,10 +433,10 @@
     pieces = tall * side * side
     return pl.pallas_call(
         functools.partial(fused_kernel, side, tall, order),
-        out_shape=jax.ShapeDtypeStruct((count, channels), jnp.bfloat16),
+        out_shape=pltpu.VMEM((count, channels), jnp.bfloat16),
         in_specs=[pl.BlockSpec(memory_space=pl.ANY)] * 4
         + [pl.BlockSpec(memory_space=pltpu.VMEM)] * 3,
-        out_specs=pl.BlockSpec(memory_space=pl.ANY),
+        out_specs=pl.BlockSpec(memory_space=pltpu.VMEM),
         scratch_shapes=[
             pltpu.VMEM((blocks, width, 2 * channels // blocks), jnp.bfloat16),
             pltpu.VMEM((HALO + count, width), jnp.bfloat16),
@@ -449,7 +445,6 @@
             pltpu.VMEM((HALO // 8, HALO + count + SPARE, LANES), jnp.float32),
             pltpu.VMEM((HALO // 8 - 1, HALO + count + SPARE, LANES), jnp.float32),
             pltpu.VMEM((7, count + SPARE, LANES), jnp.float32),
-            pltpu.VMEM((count, channels), jnp.bfloat16),
             pltpu.VMEM((count, LANES), jnp.float32),
             pltpu.VMEM((count, LANES), jnp.float32),
             pltpu.VMEM((count, LANES), jnp.float32),
@@ -459,7 +454,6 @@
             pltpu.SemaphoreType.DMA((blocks, 2 * channels // (blocks * LANES))),
             pltpu.SemaphoreType.DMA((2,)),
             pltpu.SemaphoreType.DMA((4,)),
-            pltpu.SemaphoreType.DMA((count // LEAVE,)),
         ],
         compiler_params=pltpu.CompilerParams(
             collective_id=0, has_side_effects=True, vmem_limit_bytes=56 * 1024 * 1024

time: 142 us -> 138 us (0.972)
  Pallas kernels: 139 us -> 137 us
  local copies, waits for them, and re-layouts: 3.16 us -> 1.32 us
    pallas_call x1, Pallas kernels: 139 us -> 137 us  [activated_product(): pl.pallas_call(functools.partial(fused_kernel, side, tall, order), out_sh...]
    unnamed x1, local copies, waits for them, and re-layouts: 3.16 us -> 1.32 us
where the time goes in v4:
time: 138 us
  Pallas kernels  137 us (99%)
    pallas_call x1, Pallas kernels, activated_product(): pl.pallas_call(functools.partial(fused_kernel, side, tall, order), out_sh...  137 us

profile of v4, /device:TPU:0, one launch (start us, length us, event | category | flops | bytes accessed | tf_op | source)
XLA Modules:
  0.0 138.0 jit_solution(16929358611536985272)
XLA Ops:
  0.0 136.6 %shard_map.73 = bf16[512,2048]{1,0:T(8,128)(2,1)S(1)} custom-call(bf16[512,4096]{1,0:T(8,128)(2,1)} %bitcast.5, s32[1,512]{1,0:T(1,128)} %docs_hbm.1, bf16[128,2048]{1,0:T(8,128)(2,1)} %value_hbm.1, bf16[128,2048]{1,0:T(8,128)(2,1)} %gate_hbm.1, bf16[31,2048]{1,0:T(8,128)(2,1)} %conv_ref.1, f32[1,2048]{1,0:T(1,128)} %bitcast.6, f32[1,2048]{1,0:T(1,128)} %bitcast.7), custom_call_target="tpu_custom_call" | custom-call | tf_op jit(solution)/shard_map/pallas_call | solution.py:434
  136.6 1.3 copy.9

commit v5 on v4

--- a/solution.py
+++ b/solution.py
@@ -17,7 +17,7 @@
 
 
 def plan(side, tall, channels):
-    order = dict(blocks=channels // LANES, tall_first=((1, 4, 7, 10, 13), (0, 2, 7, 8, 11, 13)), own=47)
+    order = dict(blocks=channels // LANES, after=6, tall_first=((1, 4, 7, 10, 13), (0, 2, 7, 8, 11, 13)), own=47)
     if side == 2 and tall == 4:
         order.update(along_z=(0, 4, 7), along_u=(0, 7, 9, 10), near_v=(5, 11, 12, 12), far_v=(9, 13, 14, 14), late=16)
     else:
@@ -33,8 +33,8 @@
 
 
 def fused_kernel(
-    side, tall, order, tok_hbm, docs_hbm, value_hbm, gate_hbm, conv_ref, gain_ref,
-    bias_ref, mixed, weights, tok, docs, taps, shifted, far, near_by, center,
+    side, tall, order, tok_hbm, docs_hbm, value_hbm, gate_hbm, conv_hbm, gain_hbm,
+    bias_hbm, mixed, weights, tok, docs, conv_ref, gain_ref, bias_ref, leading, trailing, taps, shifted, far, near_by, center,
     total, square, send, recv, cross, own, begin, halo
 ):
     sp, dp = lax.axis_index("sp"), lax.axis_index("dp")
@@ -47,8 +47,7 @@
     count = tok_hbm.shape[0]
     blocks = order["blocks"]
     channels = value_hbm.shape[1]
-    parts = channels // (blocks * LANES)
-    lines = (HALO + count) // 2
+    span = count // 2
     other = {"sp": sp, "dp": y * 2 + (1 - core)}
     here = (z * side + x) * side + y
 
@@ -181,14 +180,13 @@
 
     def own_copies(block):
         rows = pl.ds(pl.multiple_of((here * 2 + core) * depth, depth), depth)
-        for part in range(parts):
-            first = pl.multiple_of((block * parts + part) * LANES, LANES)
-            for half, source in enumerate((value_hbm, gate_hbm)):
-                yield pltpu.make_async_copy(
-                    source.at[:, pl.ds(first, LANES)],
-                    weights.at[block, rows, pl.ds((2 * part + half) * LANES, LANES)],
-                    own.at[block, 2 * part + half],
-                )
+        first = pl.multiple_of(block * LANES, LANES)
+        for half, source in enumerate((value_hbm, gate_hbm)):
+            yield pltpu.make_async_copy(
+                source.at[:, pl.ds(first, LANES)],
+                weights.at[block, rows, pl.ds(half * LANES, LANES)],
+                own.at[block, half],
+            )
 
     def send_own(block):
         for copy in own_copies(block):
@@ -219,34 +217,43 @@
         for copy in own_copies(block):
             copy.start()
 
-    load = pltpu.make_async_copy(tok_hbm, tok.at[pl.ds(HALO, count), :], begin.at[0])
+    load = pltpu.make_async_copy(tok_hbm, tok, begin.at[0])
     load.start()
     read = pltpu.make_async_copy(docs_hbm, docs.at[:, pl.ds(LANES, count)], begin.at[1])
     read.start()
+    small = [
+        pltpu.make_async_copy(source, target, begin.at[2 + i])
+        for i, (source, target) in enumerate(
+            ((conv_hbm, conv_ref), (gain_hbm, gain_ref), (bias_hbm, bias_ref))
+        )
+    ]
+    for copy in small:
+        copy.start()
 
     pl.semaphore_wait(barrier, greeted)
 
     following = {"sp": lax.rem(sp + 1, sp_size), "dp": dp}
-    tail = pltpu.make_async_remote_copy(
-        src_ref=tok_hbm.at[pl.ds(count - HALO, HALO), :],
-        dst_ref=tok.at[pl.ds(0, HALO), :],
-        send_sem=halo.at[0],
-        recv_sem=halo.at[1],
+    def tail(block):
+        return pltpu.make_async_remote_copy(
+            src_ref=trailing.at[block],
+            dst_ref=leading.at[block],
+            send_sem=halo.at[0, block],
+            recv_sem=halo.at[1, block],
+            device_id=following,
+            device_id_type=MESH,
+        )
+
+    docs_tail = pltpu.make_async_remote_copy(
+        src_ref=docs_hbm.at[:, pl.ds(count - LANES, LANES)],
+        dst_ref=docs.at[:, pl.ds(0, LANES)],
+        send_sem=halo.at[0, blocks],
+        recv_sem=halo.at[1, blocks],
         device_id=following,
         device_id_type=MESH,
     )
-    docs_tail = pltpu.make_async_remote_copy(
-        src_ref=docs_hbm.at[:, pl.ds(count - LANES, LANES)],
-        dst_ref=docs.at[:, pl.ds(0, LANES)],
-        send_sem=halo.at[2],
-        recv_sem=halo.at[3],
-        device_id=following,
-        device_id_type=MESH,
-    )
 
     @pl.when(sp + 1 < sp_size)
     def _():
-        tail.start()
         docs_tail.start()
 
     ahead = min(blocks, -(-order["own"] // tall))
@@ -257,18 +264,18 @@
 
     @pl.when(sp == 0)
     def _():
-        tok[pl.ds(0, HALO), :] = jnp.zeros((HALO, tok.shape[1]), tok.dtype)
+        leading[...] = jnp.zeros_like(leading)
         docs[:, pl.ds(0, LANES)] = jnp.full((1, LANES), -1, jnp.int32)
-
-    taps[pl.ds(0, KERNEL), :] = conv_ref[...].astype(jnp.float32)
 
     def prepare():
         load.wait()
         read.wait()
+        for copy in small:
+            copy.wait()
+        taps[pl.ds(0, KERNEL), :] = conv_ref[...].astype(jnp.float32)
 
         @pl.when(sp > 0)
         def _():
-            tail.wait_recv()
             docs_tail.wait_recv()
 
         column = jnp.broadcast_to(docs[...], (LANES, LANES + count)).T
@@ -283,26 +290,36 @@
         total[...] = jnp.zeros_like(total)
         square[...] = jnp.zeros_like(square)
 
-    def project(block, part, half):
-        rows = pl.ds(half * lines, lines)
-        held = weights[
-            block, :, pl.ds(pl.multiple_of(part * 2 * LANES, 2 * LANES), 2 * LANES)
-        ]
-        both = jnp.dot(tok[rows, :], held, preferred_element_type=jnp.float32)
+    def project(block, half):
+        rows = pl.ds(half * span, span)
+        both = jnp.dot(tok[rows, :], weights[block], preferred_element_type=jnp.float32)
         value = both[:, :LANES].astype(jnp.bfloat16).astype(jnp.float32)
         gate = both[:, LANES:].astype(jnp.bfloat16).astype(jnp.float32)
-        glu = (value * jax.nn.sigmoid(gate)).astype(jnp.bfloat16).astype(jnp.float32)
-        shifted[0, rows, :] = glu
-
-    def convolve(block, part, half):
-        first = pl.multiple_of((block * parts + part) * LANES, LANES)
-        lanes = pl.ds(first, LANES)
-        span = count // 2
+        glu = (value * jax.nn.sigmoid(gate)).astype(jnp.bfloat16)
+        base = lax.rem(block, 2) * (HALO // 8)
+        shifted[base, pl.ds(HALO + half * span, span), :] = glu.astype(jnp.float32)
+        if half:
+            trailing[block] = glu[span - HALO :]
+
+    def exchange(block):
+        @pl.when(sp + 1 < sp_size)
+        def _():
+            tail(block).start()
+
+    def convolve(block, half):
+        lanes = pl.ds(pl.multiple_of(block * LANES, LANES), LANES)
+        base = lax.rem(block, 2) * (HALO // 8)
+        if half == 0:
+            @pl.when(sp > 0)
+            def _():
+                tail(block).wait_recv()
+
+            shifted[base, pl.ds(0, HALO), :] = leading[block].astype(jnp.float32)
         start = half * span + HALO - 8
         kept = pl.ds(start, span + 8)
         for a in range(1, HALO // 8):
-            moved = shifted[0, pl.ds(start - 8 * a, span + 8), :]
-            shifted[a, kept, :] = moved * far[a - 1, kept, :]
+            moved = shifted[base, pl.ds(start - 8 * a, span + 8), :]
+            shifted[base + a, kept, :] = moved * far[a - 1, kept, :]
 
         @pl.loop(0, span // TILE)
         def _(tile):
@@ -313,7 +330,7 @@
                 for a in range(HALO // 8):
                     lag = 8 * a + r
                     if lag < KERNEL:
-                        moved = shifted[a, pl.ds(top + HALO - r, TILE), :]
+                        moved = shifted[base + a, pl.ds(top + HALO - r, TILE), :]
                         term = moved * taps[lag : lag + 1, lanes]
                         run = term if run is None else run + term
                 if r:
@@ -324,7 +341,7 @@
             mixed[rows, lanes] = rounded
             held = rounded.astype(jnp.float32)
 
-            @pl.when(first == 0)
+            @pl.when(block == 0)
             def _():
                 middle = jnp.mean(held, axis=-1, keepdims=True)
                 center[rows, :] = jnp.broadcast_to(middle, (TILE, LANES))
@@ -375,15 +392,10 @@
             pl.when(block == 0)(prepare)
             hand_over(many(block, pieces), block).wait_recv()
 
-        steps = [
-            (act, part, half)
-            for part in range(parts)
-            for act in (project, convolve)
-            for half in range(2)
-        ]
-        for act, part, half in steps[k * len(steps) // tall : (k + 1) * len(steps) // tall]:
-            act(block, part, half)
-
+            project(block, 1)
+        if k == 1:
+            exchange(block)
+            project(block, 0)
         if k == tall - 1:
             all_sent(block)
 
@@ -393,9 +405,12 @@
     for name, act in (("along_u", near_u), ("near_v", near_v), ("far_v", far_v)):
         for k in range(tall):
             sites.append((order[name][k], lambda block, k=k, act=act: act(block, k)))
+    assert all(offset <= order["late"] for offset, _ in sites)
     for k in range(tall):
         sites.append((order["late"] + k, lambda block, k=k: compute(block, k)))
-    assert all(offset <= order["late"] for offset, _ in sites[:-tall])
+    for half in range(2):
+        place = order["late"] + order["after"] + 1 - half
+        sites.append((place, lambda block, half=half: convolve(block, half)))
 
     def round_of(number, carry):
         for j in range(tall):
@@ -411,13 +426,16 @@
 
         return carry
 
-    rounds = blocks + (order["late"] + tall - 1) // tall
+    rounds = blocks + (order["late"] + order["after"] + tall) // tall
     lax.fori_loop(0, rounds, round_of, 0)
     finish()
 
     @pl.when(sp + 1 < sp_size)
     def _():
-        tail.wait_send()
+        @pl.loop(0, blocks)
+        def _(block):
+            tail(block).wait_send()
+
         docs_tail.wait_send()
 
 
@@ -434,15 +452,19 @@
     return pl.pallas_call(
         functools.partial(fused_kernel, side, tall, order),
         out_shape=pltpu.VMEM((count, channels), jnp.bfloat16),
-        in_specs=[pl.BlockSpec(memory_space=pl.ANY)] * 4
-        + [pl.BlockSpec(memory_space=pltpu.VMEM)] * 3,
+        in_specs=[pl.BlockSpec(memory_space=pl.ANY)] * 7,
         out_specs=pl.BlockSpec(memory_space=pltpu.VMEM),
         scratch_shapes=[
             pltpu.VMEM((blocks, width, 2 * channels // blocks), jnp.bfloat16),
-            pltpu.VMEM((HALO + count, width), jnp.bfloat16),
+            pltpu.VMEM((count, width), jnp.bfloat16),
             pltpu.VMEM((1, LANES + count), jnp.int32),
+            pltpu.VMEM(conv_weight.shape, conv_weight.dtype),
+            pltpu.VMEM((1, channels), jnp.float32),
+            pltpu.VMEM((1, channels), jnp.float32),
+            pltpu.VMEM((blocks, HALO, LANES), jnp.bfloat16),
+            pltpu.VMEM((blocks, HALO, LANES), jnp.bfloat16),
             pltpu.VMEM((HALO, channels), jnp.float32),
-            pltpu.VMEM((HALO // 8, HALO + count + SPARE, LANES), jnp.float32),
+            pltpu.VMEM((2 * (HALO // 8), HALO + count + SPARE, LANES), jnp.float32),
             pltpu.VMEM((HALO // 8 - 1, HALO + count + SPARE, LANES), jnp.float32),
             pltpu.VMEM((7, count + SPARE, LANES), jnp.float32),
             pltpu.VMEM((count, LANES), jnp.float32),
@@ -451,9 +473,9 @@
             pltpu.SemaphoreType.DMA((7, blocks)),
             pltpu.SemaphoreType.DMA((blocks, pieces)),
             pltpu.SemaphoreType.DMA((blocks,)),
-            pltpu.SemaphoreType.DMA((blocks, 2 * channels // (blocks * LANES))),
-            pltpu.SemaphoreType.DMA((2,)),
-            pltpu.SemaphoreType.DMA((4,)),
+            pltpu.SemaphoreType.DMA((blocks, 2)),
+            pltpu.SemaphoreType.DMA((5,)),
+            pltpu.SemaphoreType.DMA((2, blocks + 1)),
         ],
         compiler_params=pltpu.CompilerParams(
             collective_id=0, has_side_effects=True, vmem_limit_bytes=56 * 1024 * 1024

time: 138 us -> 137 us (level)
  Pallas kernels: 137 us -> 135 us
    pallas_call x1, Pallas kernels: 137 us -> 135 us  [activated_product(): pl.pallas_call(functools.partial(fused_kernel, side, tall, order), out_sh...]
where the time goes in v5:
time: 137 us
  Pallas kernels  135 us (99%)
    pallas_call x1, Pallas kernels, activated_product(): pl.pallas_call(functools.partial(fused_kernel, side, tall, order), out_sh...  135 us

profile of v5, /device:TPU:0, one launch (start us, length us, event | category | flops | bytes accessed | tf_op | source)
XLA Modules:
  0.0 136.5 jit_solution(17419035211926013664)
XLA Ops:
  0.0 135.2 %shard_map.73 = bf16[512,2048]{1,0:T(8,128)(2,1)S(1)} custom-call(bf16[512,4096]{1,0:T(8,128)(2,1)} %bitcast.5, s32[1,512]{1,0:T(1,128)} %docs_hbm.1, bf16[128,2048]{1,0:T(8,128)(2,1)} %value_hbm.1, bf16[128,2048]{1,0:T(8,128)(2,1)} %gate_hbm.1, bf16[31,2048]{1,0:T(8,128)(2,1)} %conv_hbm.1, f32[1,2048]{1,0:T(1,128)} %bitcast.6, f32[1,2048]{1,0:T(1,128)} %bitcast.7), custom_call_target="tpu_custom_call" | custom-call | tf_op jit(solution)/shard_map/pallas_call | solution.py:452
  135.2 1.3 copy.9

commit v6 on v5

--- a/solution.py
+++ b/solution.py
@@ -17,9 +17,9 @@
 
 
 def plan(side, tall, channels):
-    order = dict(blocks=channels // LANES, after=6, tall_first=((1, 4, 7, 10, 13), (0, 2, 7, 8, 11, 13)), own=47)
+    order = dict(blocks=channels // LANES, after=6, tall_first=((1, 4, 5, 10, 13), (1, 2, 7, 8, 11, 13)), own=34)
     if side == 2 and tall == 4:
-        order.update(along_z=(0, 4, 7), along_u=(0, 7, 9, 10), near_v=(5, 11, 12, 12), far_v=(9, 13, 14, 14), late=16)
+        order.update(along_z=(0, 4, 7), along_u=(0, 7, 7, 10), near_v=(7, 9, 11, 13), far_v=(7, 15, 16, 16), late=17)
     else:
         order.update(
             own=tall,
@@ -48,6 +48,7 @@
     blocks = order["blocks"]
     channels = value_hbm.shape[1]
     span = count // 2
+    slots = shifted.shape[0] // (HALO // 8)
     other = {"sp": sp, "dp": y * 2 + (1 - core)}
     here = (z * side + x) * side + y
 
@@ -296,7 +297,7 @@
         value = both[:, :LANES].astype(jnp.bfloat16).astype(jnp.float32)
         gate = both[:, LANES:].astype(jnp.bfloat16).astype(jnp.float32)
         glu = (value * jax.nn.sigmoid(gate)).astype(jnp.bfloat16)
-        base = lax.rem(block, 2) * (HALO // 8)
+        base = lax.rem(block, slots) * (HALO // 8)
         shifted[base, pl.ds(HALO + half * span, span), :] = glu.astype(jnp.float32)
         if half:
             trailing[block] = glu[span - HALO :]
@@ -308,7 +309,7 @@
 
     def convolve(block, half):
         lanes = pl.ds(pl.multiple_of(block * LANES, LANES), LANES)
-        base = lax.rem(block, 2) * (HALO // 8)
+        base = lax.rem(block, slots) * (HALO // 8)
         if half == 0:
             @pl.when(sp > 0)
             def _():
@@ -448,6 +449,7 @@
     channels = value_weight.shape[1]
     order = plan(side, tall, channels)
     blocks = order["blocks"]
+    slots = (order["after"] + 1) // tall + 1
     pieces = tall * side * side
     return pl.pallas_call(
         functools.partial(fused_kernel, side, tall, order),
@@ -464,7 +466,7 @@
             pltpu.VMEM((blocks, HALO, LANES), jnp.bfloat16),
             pltpu.VMEM((blocks, HALO, LANES), jnp.bfloat16),
             pltpu.VMEM((HALO, channels), jnp.float32),
-            pltpu.VMEM((2 * (HALO // 8), HALO + count + SPARE, LANES), jnp.float32),
+            pltpu.VMEM((slots * (HALO // 8), HALO + count + SPARE, LANES), jnp.float32),
             pltpu.VMEM((HALO // 8 - 1, HALO + count + SPARE, LANES), jnp.float32),
             pltpu.VMEM((7, count + SPARE, LANES), jnp.float32),
             pltpu.VMEM((count, LANES), jnp.float32),

time: 137 us -> 136 us (level)
  no operation moved by 1% of the time
where the time goes in v6:
time: 136 us; the launch traced here: 135 us
  Pallas kernels  134 us (99%)
    pallas_call x1, Pallas kernels, activated_product(): pl.pallas_call(functools.partial(fused_kernel, side, tall, order), out_sh...  134 us

profile of v6, /device:TPU:0, one launch (start us, length us, event | category | flops | bytes accessed | tf_op | source)
XLA Modules:
  0.0 135.5 jit_solution(17778011003070160180)
XLA Ops:
  0.0 134.2 %shard_map.73 = bf16[512,2048]{1,0:T(8,128)(2,1)S(1)} custom-call(bf16[512,4096]{1,0:T(8,128)(2,1)} %bitcast.5, s32[1,512]{1,0:T(1,128)} %docs_hbm.1, bf16[128,2048]{1,0:T(8,128)(2,1)} %value_hbm.1, bf16[128,2048]{1,0:T(8,128)(2,1)} %gate_hbm.1, bf16[31,2048]{1,0:T(8,128)(2,1)} %conv_hbm.1, f32[1,2048]{1,0:T(1,128)} %bitcast.6, f32[1,2048]{1,0:T(1,128)} %bitcast.7), custom_call_target="tpu_custom_call" | custom-call | tf_op jit(solution)/shard_map/pallas_call | solution.py:454
  134.2 1.3 copy.9

commit v7 on v6

--- a/solution.py
+++ b/solution.py
@@ -410,7 +410,7 @@
     for k in range(tall):
         sites.append((order["late"] + k, lambda block, k=k: compute(block, k)))
     for half in range(2):
-        place = order["late"] + order["after"] + 1 - half
+        place = order["late"] + (2 if half else order["after"] + 1)
         sites.append((place, lambda block, half=half: convolve(block, half)))
 
     def round_of(number, carry):

time: 136 us -> 135 us (level)
  no operation moved by 1% of the time
where the time goes in v7:
time: 135 us
  Pallas kernels  134 us (99%)
    pallas_call x1, Pallas kernels, activated_product(): pl.pallas_call(functools.partial(fused_kernel, side, tall, order), out_sh...  134 us

profile of v7, /device:TPU:0, one launch (start us, length us, event | category | flops | bytes accessed | tf_op | source)
XLA Modules:
  0.0 135.1 jit_solution(4703141002398436314)
XLA Ops:
  0.0 133.7 %shard_map.73 = bf16[512,2048]{1,0:T(8,128)(2,1)S(1)} custom-call(bf16[512,4096]{1,0:T(8,128)(2,1)} %bitcast.5, s32[1,512]{1,0:T(1,128)} %docs_hbm.1, bf16[128,2048]{1,0:T(8,128)(2,1)} %value_hbm.1, bf16[128,2048]{1,0:T(8,128)(2,1)} %gate_hbm.1, bf16[31,2048]{1,0:T(8,128)(2,1)} %conv_hbm.1, f32[1,2048]{1,0:T(1,128)} %bitcast.6, f32[1,2048]{1,0:T(1,128)} %bitcast.7), custom_call_target="tpu_custom_call" | custom-call | tf_op jit(solution)/shard_map/pallas_call | solution.py:454
  133.7 1.3 copy.9
